TPU v7x, 32 devices: a whole 2x2x4 slice. The times are simulated.
32 devices in a mesh: sp: 8 (over z, x), tp: 4 (over y, core).
Axes of the slice: x: 2, y: 2, z: 4, core: 2. Of those that a mesh axis runs over, the one named last changes fastest.
Arguments:
- queries: bfloat16 [1024, 2048], P('sp', 'tp'), may hold values from -18 to 90
- projected_key_rows: bfloat16 [1024, 1024], P('sp', 'tp'), may hold values from -18 to 90
- projected_value_rows: bfloat16 [1024, 1024], P('sp', 'tp'), may hold values from -6 to 6
- query_gain: float32 [64], replicated, may hold values from 1 to 6
- key_norm_gain: float32 [64], replicated, may hold values from 1 to 6
- residual: bfloat16 [1024, 2048], P('sp', 'tp'), may hold values from -54 to 54
- out_weight: bfloat16 [2048, 2048], P('tp'), may hold values from -1 to 1
- norm_gain: float32 [2048], P('tp'), may hold values from 0.28 to 4.68
- expert_ids: int32 [1024, 2], P('sp'), may hold values from 0 to 7, as said below
- route_weights: float32 [1024, 2], P('sp'), may hold values from 0.2 to 1
- gate_weight: bfloat16 [8, 2048, 4096], P('sp', None, 'tp'), may hold values from -0.125 to 0.125
- up_weight: bfloat16 [8, 2048, 4096], P('sp', None, 'tp'), may hold values from -0.125 to 0.125
- down_weight: bfloat16 [8, 4096, 2048], P('sp', 'tp'), may hold values from -0.25 to 0.25
- final_gain: float32 [2048], P('tp'), may hold values from 0.1 to 1.9
Outputs:
- layer_out: bfloat16 [1024, 2048], P('sp', 'tp')
Inputs may be any that keep to these rules, and one draw needn't show every extreme that they name: `expert_ids`: each row names two different experts of one group, the group of expert e being e // 4. In every aligned block of 128 rows each group is named by the same number of rows, no expert is named by more than 64 rows, one expert of every group is named by exactly 64 rows, and one expert is named by 64 rows of every block.
All inputs are finite; a program needn't handle non-finite values.
Results may differ from a plain program's by a relative error of at most 0.019.
The roundings to bfloat16 on the way count: a program that leaves them out, or rounds other values in their place, can miss the bound.
Values may be sent and summed in bfloat16 or wider, within the bound.
A program may use at most 64 MiB of HBM per device.

v0:
```python
from functools import reduce

import jax
import jax.numpy as jnp
from jax import lax
from jax.sharding import PartitionSpec as P

D = 2048
HEAD_DIM = 64
GRID_W = 64
TOPK = 2


theta_base = 10000.0
norm_epsilon = 1e-06
residual_scale = 8.0**0.25
far_below = -1e30


def rope_line(halves, angles):
    pair_count = angles.shape[-1]
    first_half = halves[..., :pair_count]
    second_half = halves[..., pair_count:]
    cosine = jnp.cos(angles)[:, None, :]
    sine_part = jnp.sin(angles)[:, None, :]
    return jnp.concatenate(
        [
            first_half * cosine - second_half * sine_part,
            first_half * sine_part + second_half * cosine,
        ],
        -1,
    )


def rotary_over_grid(rows_by_head, token_positions):
    head_size = rows_by_head.shape[-1]
    frequency = theta_base ** (
        -jnp.arange(0, head_size // 2, 2, dtype=jnp.float32) / (head_size // 2)
    )
    grid_row = (token_positions // GRID_W).astype(jnp.float32)
    grid_col = (token_positions % GRID_W).astype(jnp.float32)
    row_part = rope_line(
        rows_by_head[..., : head_size // 2], grid_row[:, None] * frequency[None, :]
    )
    col_part = rope_line(
        rows_by_head[..., head_size // 2 :], grid_col[:, None] * frequency[None, :]
    )
    return jnp.concatenate([row_part, col_part], -1)


def normalize_heads(token_rows, gain_row, head_count):
    shaped = token_rows.astype(jnp.float32).reshape(token_rows.shape[0], head_count, -1)
    scaled = shaped * lax.rsqrt(jnp.mean(shaped * shaped, -1, keepdims=True) + norm_epsilon)
    return scaled * gain_row[None, None, :]


def norm_features(feature_rows, gain_row, feature_total):
    row_sums = jnp.sum(feature_rows, 0)
    squares = jnp.sum(feature_rows * feature_rows, 0)
    row_sums, squares = lax.psum((row_sums, squares), "tp")
    center = row_sums / feature_total
    spread = squares / feature_total - center * center
    return (
        (feature_rows - center[None, :])
        * lax.rsqrt(spread + norm_epsilon)[None, :]
        * gain_row[:, None]
    )


def per_device(
    queries,
    projected_key_rows,
    projected_value_rows,
    query_gain,
    key_norm_gain,
    residual,
    out_weight,
    norm_gain,
    expert_ids,
    route_weights,
    gate_weight,
    up_weight,
    down_weight,
    final_gain,
):
    token_count = queries.shape[0]
    query_heads = queries.shape[1] // HEAD_DIM
    key_heads = projected_key_rows.shape[1] // HEAD_DIM
    queries_per_group = query_heads // key_heads
    token_positions = lax.axis_index("sp") * token_count + jnp.arange(token_count, dtype=jnp.int32)
    queries_after_rotation = rotary_over_grid(
        normalize_heads(queries, query_gain, query_heads), token_positions
    ).astype(jnp.bfloat16)
    keys_after_rotation = rotary_over_grid(
        normalize_heads(projected_key_rows, key_norm_gain, key_heads), token_positions
    ).astype(jnp.bfloat16)
    packed = jnp.concatenate(
        [keys_after_rotation, projected_value_rows.reshape(token_count, key_heads, HEAD_DIM)], -1
    ).reshape(token_count, key_heads * 2 * HEAD_DIM)
    grouped_query_heads = (
        queries_after_rotation.reshape(token_count, key_heads, queries_per_group, HEAD_DIM)
        .transpose(1, 2, 0, 3)
        .reshape(key_heads, queries_per_group * token_count, HEAD_DIM)
    )
    score_scale = HEAD_DIM ** (-0.5)
    query_total = queries_per_group * token_count
    section = lax.all_gather(packed, "sp", axis=0, tiled=True)
    running_max = jnp.full((key_heads, query_total), far_below, jnp.float32)
    opened = section.reshape(section.shape[0], key_heads, 2 * HEAD_DIM)
    scores = (
        jnp.einsum(
            "hqd,khd->hqk",
            grouped_query_heads,
            opened[:, :, :HEAD_DIM],
            preferred_element_type=jnp.float32,
        )
        * score_scale
    )
    new_peak = jnp.maximum(running_max, jnp.max(scores, -1))
    weights = jnp.exp(scores - new_peak[:, :, None])
    running_sum = jnp.sum(weights, -1)
    running_out = jnp.einsum(
        "hqk,khd->hqd",
        weights.astype(jnp.bfloat16),
        opened[:, :, HEAD_DIM:],
        preferred_element_type=jnp.float32,
    )
    running_max, running_sum, running_out = (new_peak, running_sum, running_out)
    attended = (running_out / running_sum[:, :, None]).astype(jnp.bfloat16)
    attended = (
        attended.reshape(key_heads, queries_per_group, token_count, HEAD_DIM)
        .transpose(2, 0, 1, 3)
        .reshape(token_count, query_heads * HEAD_DIM)
    )
    local_width = residual.shape[1]
    columns = out_weight
    mixed_rows = lax.psum_scatter(
        lax.dot_general(
            columns, attended, (((0,), (1,)), ((), ())), preferred_element_type=jnp.float32
        ).astype(jnp.bfloat16),
        "tp",
        scatter_dimension=0,
        tiled=True,
    ).astype(jnp.float32)
    pre_norm = residual_scale * residual.astype(jnp.float32).T + mixed_rows
    normed = norm_features(pre_norm, norm_gain, D).astype(jnp.bfloat16)
    expert_count = lax.axis_size("sp")
    capacity = 4 * token_count // expert_count
    row_total = expert_count * capacity
    flat_ids = expert_ids.reshape(-1)
    marked = (flat_ids[:, None] == jnp.arange(expert_count, dtype=jnp.int32)[None, :]).astype(
        jnp.int32
    )
    earlier = jnp.cumsum(marked, 0) - marked
    places = (flat_ids * capacity + jnp.sum(earlier * marked, 1)).reshape(token_count, TOPK)
    lane_index = jnp.arange(row_total, dtype=jnp.int32)
    selectors = [
        (places[:, route_rank : route_rank + 1] == lane_index[None, :]).astype(jnp.bfloat16)
        for route_rank in range(TOPK)
    ]
    dispatch = reduce(jnp.add, selectors)
    gate_local = gate_weight[0]
    up_local = up_weight[0]
    down_local = down_weight[0]
    outgoing = lax.dot_general(
        dispatch, normed, (((0,), (1,)), ((), ())), preferred_element_type=jnp.float32
    ).astype(jnp.bfloat16)
    arrived = lax.all_to_all(
        outgoing.reshape(expert_count, capacity, local_width),
        "sp",
        split_axis=0,
        concat_axis=0,
        tiled=True,
    ).reshape(row_total, local_width)
    section = lax.all_gather(arrived, "tp", axis=1, tiled=True)
    gate_sum = jnp.dot(section, gate_local, preferred_element_type=jnp.float32)
    up_sum = jnp.dot(section, up_local, preferred_element_type=jnp.float32)
    hidden = (jax.nn.silu(gate_sum) * up_sum).astype(jnp.bfloat16)
    columns = down_local
    expert_out = lax.psum_scatter(
        lax.dot_general(
            columns, hidden, (((0,), (1,)), ((), ())), preferred_element_type=jnp.float32
        ).astype(jnp.bfloat16),
        "tp",
        scatter_dimension=0,
        tiled=True,
    )
    returned = lax.all_to_all(
        expert_out.reshape(local_width, expert_count, capacity),
        "sp",
        split_axis=1,
        concat_axis=1,
        tiled=True,
    ).reshape(local_width, row_total)
    combined = jnp.zeros((local_width, token_count), jnp.float32)
    for route_rank in range(TOPK):
        chosen = lax.dot_general(
            returned,
            selectors[route_rank],
            (((1,), (1,)), ((), ())),
            preferred_element_type=jnp.float32,
        )
        combined = combined + chosen * route_weights[:, route_rank][None, :]
    second_sum = residual_scale * normed.astype(jnp.float32) + combined
    return norm_features(second_sum, final_gain, D).T.astype(jnp.bfloat16)


def solution(mesh):
    in_specs = (
        P("sp", "tp"),
        P("sp", "tp"),
        P("sp", "tp"),
        P(),
        P(),
        P("sp", "tp"),
        P("tp", None),
        P("tp"),
        P("sp", None),
        P("sp", None),
        P("sp", None, "tp"),
        P("sp", None, "tp"),
        P("sp", "tp", None),
        P("tp"),
    )
    out_specs = P("sp", "tp")
    return jax.shard_map(
        per_device, mesh=mesh, in_specs=in_specs, out_specs=out_specs, check_vma=False
    )
```

profile of v0, /device:TPU:0, one launch (start us, length us, event | category | flops | bytes accessed | tf_op | source)
XLA Modules:
  0.0 209.7 jit_solution(3007069951881743205)
XLA Ops:
  6.6 1.1 copy.42
  7.7 0.7 fusion.43
  8.7 1.0 copy.43
  9.7 0.6 copy-done.2
  10.4 1.0 copy.40
  11.5 0.7 fusion.38
  12.3 40.3 %all-gather.3.cloned.1.call-done = bf16[1024,512]{0,1:T(8,128)(2,1)} async-done(((bf16[128,512]{0,1:T(8,128)(2,1)}), bf16[1024,512]{0,1:T(8,128)(2,1)}) %all-gather.3.cloned.1.call-update) | async-done | bytes 1048592 | tf_op jit(solution)/shard_map/all_gather | solution.py:107
  52.6 2.0 multiply_reduce_fusion
  54.6 0.9 fusion.6
  55.5 0.9 fusion.29
  56.5 1.3 fusion.14
  59.5 19.2 %reduce-scatter.3.cloned.1.call-done = bf16[512,128]{0,1:T(8,128)(2,1)} async-done(((bf16[2048,128]{0,1:T(8,128)(2,1)}), bf16[512,128]{0,1:T(8,128)(2,1)}) %reduce-scatter.3.cloned.1.call-update) | async-done | bytes 131088 | tf_op jit(solution)/shard_map/reduce_scatter | solution.py:137
  78.7 1.0 fusion.41
  79.7 5.8 %all-reduce.1 = (f32[128]{0:T(128)S(1)}, f32[128]{0:T(128)S(1)}) all-reduce(f32[128]{0:T(128)S(1)} %get-tuple-element.8, f32[128]{0:T(128)S(1)} %get-tuple-element.7), channel_id=1, replica_groups=mesh['sp'=8,'tp'=4] {'tp'}, use_global_device_ids=true, to_apply=%region_8.9 | all-reduce | flops 256 | bytes 2048 | tf_op jit(solution)/shard_map/psum | solution.py:60
  85.5 1.3 convolution_convert_fusion.1
  86.8 19.8 %all_to_all.10 = bf16[8,64,512]{2,1,0:T(8,128)(2,1)} all-to-all(bf16[8,64,512]{2,1,0:T(8,128)(2,1)S(1)} %bitcast.97), channel_id=1, replica_groups=mesh['sp'=8,'tp'=4] {'sp'}, dimensions={0} | all-to-all | bytes 1048576 | tf_op jit(solution)/shard_map/all_to_all | solution.py:168
  106.7 20.8 %all-gather.5.cloned.1.call-done = bf16[512,2048]{1,0:T(8,128)(2,1)} async-done(((bf16[512,512]{1,0:T(8,128)(2,1)}), bf16[512,2048]{1,0:T(8,128)(2,1)}) %all-gather.5.cloned.1.call-update) | async-done | bytes 2097168 | tf_op jit(solution)/shard_map/all_gather | solution.py:175
  127.5 6.5 %fusion.4 = f32[512,1024]{1,0:T(8,128)} fusion(bf16[512,2048]{1,0:T(8,128)(2,1)} %all-gather.5.cloned.1.call-done, bf16[1,2048,1024]{2,1,0:T(8,128)(2,1)} %param.24), kind=kOutput, calls=%fused_computation.4 | convolution fusion | flops 2147483648 | bytes 8388608 | tf_op jit(solution)/shard_map/dot_general | solution.py:176
  134.0 10.6 %fusion.11 = bf16[2048,512]{0,1:T(8,128)(2,1)} fusion(bf16[1,1024,2048]{2,1,0:T(8,128)(2,1)} %param.26, f32[512,1024]{1,0:T(8,128)} %fusion.4, bf16[512,2048]{1,0:T(8,128)(2,1)} %all-gather.5.cloned.1.call-done, bf16[1,2048,1024]{2,1,0:T(8,128)(2,1)} %param.25), kind=kOutput, calls=%fused_computation.11 | convolution fusion | flops 4299161600 | bytes 14680064 | tf_op jit(solution)/shard_map/dot_general | solution.py:181
  144.6 31.3 %reduce-scatter.5.cloned.1.call-done = bf16[512,512]{0,1:T(8,128)(2,1)} async-done(((bf16[2048,512]{0,1:T(8,128)(2,1)}), bf16[512,512]{0,1:T(8,128)(2,1)}) %reduce-scatter.5.cloned.1.call-update) | async-done | bytes 524304 | tf_op jit(solution)/shard_map/reduce_scatter | solution.py:180
  175.9 5.5 %all-to-all-start.1 = ((bf16[512,8,64]{0,2,1:T(8,128)(2,1)}), bf16[512,8,64]{0,2,1:T(8,128)(2,1)S(1)}, u32[]{:S(2)}, u32[]{:S(2)}) async-start(bf16[512,8,64]{0,2,1:T(8,128)(2,1)} %bitcast.96), calls=%async_computation.3 | async-start | bytes 1048576 | tf_op jit(solution)/shard_map/all_to_all | solution.py:188
  181.5 14.3 %all-to-all-done.1 = bf16[512,8,64]{0,2,1:T(8,128)(2,1)S(1)} async-done(((bf16[512,8,64]{0,2,1:T(8,128)(2,1)}), bf16[512,8,64]{0,2,1:T(8,128)(2,1)S(1)}, u32[]{:S(2)}, u32[]{:S(2)}) %all-to-all-start.1) | async-done | bytes 524320 | tf_op jit(solution)/shard_map/all_to_all | solution.py:188
  196.5 5.9 %all-reduce = (f32[128]{0:T(128)S(1)}, f32[128]{0:T(128)S(1)}) all-reduce(f32[128]{0:T(128)S(1)} %get-tuple-element.6, f32[128]{0:T(128)S(1)} %get-tuple-element.5), channel_id=1, replica_groups=mesh['sp'=8,'tp'=4] {'tp'}, use_global_device_ids=true, to_apply=%region_16.17 | all-reduce | flops 256 | bytes 2048 | tf_op jit(solution)/shard_map/psum | solution.py:60
  202.4 0.8 fusion.47
  (58 shorter events, 2.9 us)
Async XLA Ops:
  6.5 50.0 %copy-start = (bf16[512,2048]{1,0:T(8,128)(2,1)S(1)}, bf16[512,2048]{1,0:T(8,128)(2,1)}, u32[]{:S(2)}) copy-start(bf16[512,2048]{1,0:T(8,128)(2,1)} %param.20) | copy-start | bytes 6291460
  6.5 46.1 %all-gather.3.cloned.1.call-start = ((), (), s32[]{:S(2)}) async-start(), calls=%async_computation.4 | async-start | bytes 1179648 | tf_op jit(solution)/shard_map/all_gather | solution.py:107
  9.7 0.7 copy-start.2
  10.3 68.3 %reduce-scatter.3.cloned.1.call-start = ((), (), s32[]{:S(2)}) async-start(), calls=%async_computation.5 | async-start | bytes 655360 | tf_op jit(solution)/shard_map/reduce_scatter | solution.py:137
  52.6 2.9 %copy-start.1 = (bf16[1024,512]{0,1:T(8,128)(2,1)S(1)}, bf16[1024,512]{0,1:T(8,128)(2,1)}, u32[]{:S(2)}) copy-start(bf16[1024,512]{0,1:T(8,128)(2,1)} %all-gather.3.cloned.1.call-done) | copy-start | bytes 3145732
  55.5 2.4 %copy-start.5 = (s32[128,2]{0,1:T(2,128)S(1)}, s32[128,2]{0,1:T(2,128)}, u32[]{:S(2)}) copy-start(s32[128,2]{0,1:T(2,128)} %param.22) | copy-start | bytes 3076
  55.5 23.2 %copy-start.3 = (bf16[128,512]{1,0:T(8,128)(2,1)S(1)}, bf16[128,512]{1,0:T(8,128)(2,1)}, u32[]{:S(2)}) copy-start(bf16[128,512]{1,0:T(8,128)(2,1)} %param.19) | copy-start | bytes 393220
  55.5 30.0 %copy-start.8 = (f32[512]{0:T(512)S(1)}, f32[512]{0:T(512)}, u32[]{:S(2)}) copy-start(f32[512]{0:T(512)} %param.21) | copy-start | bytes 6148
  57.8 69.7 %all-gather.5.cloned.1.call-start = ((), (), s32[]{:S(2)}) async-start(), calls=%async_computation.6 | async-start | bytes 2621440 | tf_op jit(solution)/shard_map/all_gather | solution.py:175
  106.7 69.3 %reduce-scatter.5.cloned.1.call-start = ((), (), s32[]{:S(2)}) async-start(), calls=%async_computation.7 | async-start | bytes 2621440 | tf_op jit(solution)/shard_map/reduce_scatter | solution.py:180
  134.0 47.4 %copy-start.7 = (f32[128,2]{0,1:T(2,128)S(1)}, f32[128,2]{0,1:T(2,128)}, u32[]{:S(2)}) copy-start(f32[128,2]{0,1:T(2,128)} %param.23) | copy-start | bytes 3076
  134.0 62.0 %copy-start.4 = (bf16[512,128]{0,1:T(8,128)(2,1)S(1)}, bf16[512,128]{0,1:T(8,128)(2,1)}, u32[]{:S(2)}) copy-start(bf16[512,128]{0,1:T(8,128)(2,1)} %reduce-scatter.3.cloned.1.call-done) | copy-start | bytes 393220
  144.6 57.8 %copy-start.6 = (f32[512]{0:T(512)S(1)}, f32[512]{0:T(512)}, u32[]{:S(2)}) copy-start(f32[512]{0:T(512)} %param.27) | copy-start | bytes 6148
  175.9 19.8 %all-to-all-start.1 = ((bf16[512,8,64]{0,2,1:T(8,128)(2,1)}), bf16[512,8,64]{0,2,1:T(8,128)(2,1)S(1)}, u32[]{:S(2)}, u32[]{:S(2)}) async-start(bf16[512,8,64]{0,2,1:T(8,128)(2,1)} %bitcast.96), calls=%async_computation.3 | async-start | bytes 1048576 | tf_op jit(solution)/shard_map/all_to_all | solution.py:188
Sparse Core Ops, SparseCore 0:
  10.5 42.1 all-gather.2
  57.9 20.6 reduce-scatter.2
  106.8 20.7 all-gather.4
  144.7 31.1 reduce-scatter.4
where the time goes:
time: 210 us
  waiting for transfers between devices  126 us (60%)
  blocking collectives  31.5 us (15%)
  matrix products  23.2 us (11%)
  between operations  13.4 us (6%)
  starting transfers between devices  5.64 us (3%)
  other arithmetic  5.31 us (3%)
  local copies, waits for them, and re-layouts  4.61 us (2%)
    all_gather x1, waiting for transfers between devices, per_device(): section = lax.all_gather(packed, 'sp', axis=0, tiled=True)  40.3 us
    reduce_scatter x1, waiting for transfers between devices, per_device(): lax.psum_scatter(lax.dot_general(columns, hidden, (((0,), (1,)), ((), ())...  31.3 us
    all_gather x1, waiting for transfers between devices, per_device(): section = lax.all_gather(arrived, 'tp', axis=1, tiled=True)  20.8 us
    all_to_all x1, blocking collectives, per_device(): lax.all_to_all(outgoing.reshape(expert_count, capacity, local_width), 'sp...  19.8 us
    reduce_scatter x1, waiting for transfers between devices, per_device(): lax.psum_scatter(lax.dot_general(columns, attended, (((0,), (1,)), ((), (...  19.2 us
    all_to_all x1, waiting for transfers between devices, per_device(): lax.all_to_all(expert_out.reshape(local_width, expert_count, capacity), '...  14.3 us
    psum x2, blocking collectives, norm_features(): row_sums, squares = lax.psum((row_sums, squares), 'tp')  11.7 us
    dot_general x1, matrix products, per_device(): lax.dot_general(columns, hidden, (((0,), (1,)), ((), ())), preferred_elem...  10.6 us
  transfers between devices with their start and end apart: 5, of which 5 were waited for; matrix products, arithmetic and copies ran while one was open for 2% of the time, Pallas kernels for 0%

commit v1 on v0

v1 whole, which is shorter than its diff:
```python
import jax
import jax.numpy as jnp
from jax import lax
from jax.experimental import pallas as pl
from jax.experimental.pallas import tpu as pltpu
from jax.sharding import PartitionSpec as P

D = 2048
HEAD_DIM = 64
GRID_W = 64
TOPK = 2


theta_base = 10000.0
norm_epsilon = 1e-06
residual_scale = 8.0**0.25
far_below = -1e30
MESH = pl.DeviceIdType.MESH


def rope_line(halves, angles):
    pair_count = angles.shape[-1]
    first_half = halves[..., :pair_count]
    second_half = halves[..., pair_count:]
    cosine = jnp.cos(angles)[:, None, :]
    sine_part = jnp.sin(angles)[:, None, :]
    return jnp.concatenate(
        [
            first_half * cosine - second_half * sine_part,
            first_half * sine_part + second_half * cosine,
        ],
        -1,
    )


def rotary_over_grid(rows_by_head, token_positions):
    head_size = rows_by_head.shape[-1]
    frequency = theta_base ** (
        -jnp.arange(0, head_size // 2, 2, dtype=jnp.float32) / (head_size // 2)
    )
    grid_row = (token_positions // GRID_W).astype(jnp.float32)
    grid_col = (token_positions % GRID_W).astype(jnp.float32)
    row_part = rope_line(
        rows_by_head[..., : head_size // 2], grid_row[:, None] * frequency[None, :]
    )
    col_part = rope_line(
        rows_by_head[..., head_size // 2 :], grid_col[:, None] * frequency[None, :]
    )
    return jnp.concatenate([row_part, col_part], -1)


def normalize_heads(token_rows, gain_row, head_count):
    shaped = token_rows.astype(jnp.float32).reshape(token_rows.shape[0], head_count, -1)
    scaled = shaped * lax.rsqrt(jnp.mean(shaped * shaped, -1, keepdims=True) + norm_epsilon)
    return scaled * gain_row[None, None, :]


def ring_gather(packed, group, group_minor):
    rows, width = packed.shape
    pieces = 4
    piece = rows // pieces
    half = group // 2
    major = group // group_minor

    def place_of(index):
        high, low = index // group_minor, lax.rem(index, group_minor)
        if group_minor == 1:
            return high
        back = major - 1 - high
        odd = lax.rem(back, 2)
        inner = (low - 1) * (1 - odd) + (group_minor - 1 - low) * odd
        first = jnp.where(low == 0, 1, 0)
        return first * high + (1 - first) * (major + back * (group_minor - 1) + inner)

    def device_at(place):
        if group_minor == 1:
            return place
        first = jnp.where(place < major, 1, 0)
        rest = jnp.maximum(place - major, 0)
        back = rest // (group_minor - 1)
        inner = lax.rem(rest, group_minor - 1)
        odd = lax.rem(back, 2)
        low = 1 + inner * (1 - odd) + (group_minor - 2 - inner) * odd
        other = (major - 1 - back) * group_minor + low
        return first * (place * group_minor) + (1 - first) * other

    def kernel(mine_ref, all_ref, send_sem, recv_sem, own_sem):
        me = lax.axis_index("sp")
        spot = place_of(me)
        right = device_at(lax.rem(spot + 1, group))
        left = device_at(lax.rem(spot + group - 1, group))
        barrier = pltpu.get_barrier_semaphore()
        for neighbour in (left, right):
            pl.semaphore_signal(
                barrier, inc=1, device_id={"sp": neighbour}, device_id_type=MESH
            )
        pl.semaphore_wait(barrier, 2)
        own = pltpu.make_async_copy(mine_ref, all_ref.at[0], own_sem)
        own.start()
        copies = {}
        for hop in range(1, half + 1):
            for part in range(pieces):
                span = pl.ds(part * piece, piece)
                for way in range(2):
                    if hop == half and (part < pieces // 2) != (way == 0):
                        continue
                    if hop > 1:
                        copies[way, hop - 1, part].wait_recv()
                    source_slot = (hop - 1) if way == 0 else (group - hop + 1)
                    target_slot = hop if way == 0 else group - hop
                    source = mine_ref.at[span] if hop == 1 else all_ref.at[source_slot, span]
                    copy = pltpu.make_async_remote_copy(
                        src_ref=source,
                        dst_ref=all_ref.at[target_slot, span],
                        send_sem=send_sem.at[way, hop - 1, part],
                        recv_sem=recv_sem.at[way, hop - 1, part],
                        device_id={"sp": right if way == 0 else left},
                        device_id_type=MESH,
                    )
                    copy.start()
                    copies[way, hop, part] = copy
        for way, hop, part in copies:
            if hop == half or (hop == half - 1 and (way, half, part) not in copies):
                copies[way, hop, part].wait_recv()
        for copy in copies.values():
            copy.wait_send()
        own.wait()

    return pl.pallas_call(
        kernel,
        out_shape=jax.ShapeDtypeStruct((group, rows, width), packed.dtype),
        in_specs=[pl.BlockSpec(memory_space=pltpu.VMEM)],
        out_specs=pl.BlockSpec(memory_space=pltpu.VMEM),
        scratch_shapes=[
            pltpu.SemaphoreType.DMA((2, half, pieces)),
            pltpu.SemaphoreType.DMA((2, half, pieces)),
            pltpu.SemaphoreType.DMA,
        ],
        compiler_params=pltpu.CompilerParams(
            collective_id=0, has_side_effects=True, vmem_limit_bytes=24 << 20
        ),
    )(packed)


def after_attention(
    attended, out_weight, residual, norm_gain, places, route_weights, gate_weight, up_weight,
    down_weight, final_gain, experts, shards,
):
    token_count, width = residual.shape
    lines = shards // 2
    row_total = TOPK * 2 * token_count
    capacity = row_total // experts
    groups = 4
    group_rows = row_total // groups
    group_experts = experts // groups
    halves = 2
    half_rows = row_total // halves
    hidden_units = gate_weight.shape[2]
    tile = min(256, hidden_units)
    feature_total = width * shards
    places_across = places.T
    bf16, f32 = jnp.bfloat16, jnp.float32

    def kernel(
        att_ref, ow_ref, res_ref, gain_ref, at_ref, across_ref, rw_ref, gate_hbm, up_hbm, down_hbm,
        last_gain_ref, out_ref,
        gate_v, up_v, down_v, weight_sem,
        mix_send, mix_pair, line_send, line_recv, mix_sem, line_sem,
        stat_send, stat_recv, stat_sem,
        outgoing, routed, out_sem, fwd_sem, cross_sem, relay_sem,
        hidden, part_send, part_pair, sum_send, sum_recv, own_sum, part_sem, sum_sem,
        result, returned, back_sem,
    ):
        me_s = lax.axis_index("sp")
        me_t = lax.axis_index("tp")
        line = me_t // 2
        core = lax.rem(me_t, 2)
        partner = line * 2 + 1 - core

        def line_at(step):
            return lax.rem(line + step, lines)

        barrier = pltpu.get_barrier_semaphore()
        for step in range(1, experts):
            pl.semaphore_signal(
                barrier, inc=1, device_id={"sp": lax.rem(me_s + step, experts)},
                device_id_type=MESH,
            )
        for step in range(1, shards):
            pl.semaphore_signal(
                barrier, inc=1, device_id={"tp": lax.rem(me_t + step, shards)},
                device_id_type=MESH,
            )
        loads = [
            pltpu.make_async_copy(src.at[0], dst, weight_sem.at[i])
            for i, (src, dst) in enumerate(
                ((gate_hbm, gate_v), (up_hbm, up_v), (down_hbm, down_v))
            )
        ]
        for load in loads:
            load.start()
        sent = []

        def push(source, target, sems, index, device):
            copy = pltpu.make_async_remote_copy(
                src_ref=source, dst_ref=target,
                send_sem=sems.at[(0,) + index], recv_sem=sems.at[(1,) + index],
                device_id=device, device_id_type=MESH,
            )
            copy.start()
            sent.append(copy)
            return copy

        attended_rows = att_ref[...]

        def mix(shard):
            return jnp.dot(
                attended_rows,
                ow_ref[:, pl.ds(pl.multiple_of(shard * width, width), width)],
                preferred_element_type=f32,
            )

        for step in range(lines):
            mix_send[step] = mix(line_at(step) * 2 + 1 - core).astype(bf16)
        pl.semaphore_wait(barrier, experts + shards - 2)
        pair = {}
        for step in list(range(1, lines)) + [0]:
            pair[step] = push(
                mix_send.at[step], mix_pair.at[step], mix_sem, (step,), {"tp": partner}
            )
        across = {}
        for step in range(1, lines):
            mine = mix(line_at(step) * 2 + core)
            pair[step].wait_recv()
            line_send[step - 1] = (mine + mix_pair[step].astype(f32)).astype(bf16)
            across[step] = push(
                line_send.at[step - 1], line_recv.at[step - 1], line_sem, (step - 1,),
                {"tp": line_at(step) * 2 + core},
            )
        total = mix(me_t)
        pair[0].wait_recv()
        total = total + mix_pair[0].astype(f32)
        total = total + residual_scale * res_ref[...].astype(f32)
        for step in range(1, lines):
            across[step].wait_recv()
            total = total + line_recv[step - 1].astype(f32)

        lane = lax.broadcasted_iota(jnp.int32, (token_count, 128), 1)

        def normalize(values, gain, turn):
            sums = jnp.sum(values, 1, keepdims=True)
            squares = jnp.sum(values * values, 1, keepdims=True)
            both = jnp.where(lane == 0, sums, jnp.where(lane == 1, squares, 0.0)).T[:8]
            stat_send[turn] = both
            stats = [
                push(
                    stat_send.at[turn], stat_recv.at[turn, step - 1], stat_sem,
                    (turn, step - 1), {"tp": lax.rem(me_t + step, shards)},
                )
                for step in range(1, shards)
            ]
            for step in range(1, shards):
                stats[step - 1].wait_recv()
                both = both + stat_recv[turn, step - 1]
            columns = jnp.concatenate([both] * 16, 0).T
            center = columns[:, 0:1] / feature_total
            spread = columns[:, 1:2] / feature_total - center * center
            return (values - center) * lax.rsqrt(spread + norm_epsilon) * gain

        normed = normalize(total, gain_ref[...], 0).astype(bf16)
        row_index = lax.broadcasted_iota(jnp.int32, (row_total, token_count), 0)
        picks = jnp.where(
            (row_index == across_ref[0:1, :]) | (row_index == across_ref[1:2, :]), 1.0, 0.0
        ).astype(bf16)
        spread_rows = jnp.dot(picks, normed, preferred_element_type=f32).astype(bf16)
        outgoing[...] = spread_rows
        routed[me_t, pl.ds(0, capacity)] = spread_rows[:capacity]
        arrivals = {}
        for step in range(1, experts):
            rows = pl.ds(step * capacity, capacity)
            arrivals[step] = push(
                outgoing.at[rows], routed.at[me_t, rows], out_sem, (step,),
                {"sp": lax.rem(me_s + step, experts)},
            )
        forwards, crossings, relays = {}, {}, {}

        def forward(group):
            for step in range(group * group_experts, (group + 1) * group_experts):
                if step > 0:
                    arrivals[step].wait_recv()
            rows = pl.ds(group * group_rows, group_rows)
            block = routed.at[me_t, rows]
            for step in range(1, lines):
                crossings[group, step] = push(
                    block, block, cross_sem, (group, step - 1),
                    {"tp": line_at(step) * 2 + core},
                )
            forwards[group] = push(block, block, fwd_sem, (group,), {"tp": partner})

        def relay(group):
            rows = pl.ds(group * group_rows, group_rows)
            for step in range(1, lines):
                crossings[group, step].wait_recv()
                block = routed.at[line_at(lines - step) * 2 + core, rows]
                relays[group, step] = push(
                    block, block, relay_sem, (group, step - 1), {"tp": partner}
                )

        def settle(group):
            forwards[group].wait_recv()
            for step in range(1, lines):
                relays[group, step].wait_recv()

        def expand(half):
            rows = pl.ds(half * half_rows, half_rows)

            def one_tile(index, carry):
                cols = pl.ds(pl.multiple_of(index * tile, tile), tile)
                gate_sum = jnp.zeros((half_rows, tile), f32)
                up_sum = jnp.zeros((half_rows, tile), f32)
                for shard in range(shards):
                    block = routed[shard, rows]
                    deep = pl.ds(shard * width, width)
                    gate_sum += jnp.dot(block, gate_v[deep, cols], preferred_element_type=f32)
                    up_sum += jnp.dot(block, up_v[deep, cols], preferred_element_type=f32)
                hidden[rows, cols] = (
                    gate_sum / (1.0 + jnp.exp(-gate_sum)) * up_sum
                ).astype(bf16)
                return carry

            lax.fori_loop(0, hidden_units // tile, one_tile, 0)

        def down(half, shard):
            return jnp.dot(
                hidden[pl.ds(half * half_rows, half_rows)],
                down_v[:, pl.ds(pl.multiple_of(shard * width, width), width)],
                preferred_element_type=f32,
            )

        parts, sums = {}, {}

        def shrink(half):
            for step in list(range(1, lines)) + [0]:
                part_send[half, step] = down(half, line_at(step) * 2 + 1 - core).astype(bf16)
                parts[half, step] = push(
                    part_send.at[half, step], part_pair.at[half, step], part_sem, (half, step),
                    {"tp": partner},
                )
            for step in range(1, lines):
                mine = down(half, line_at(step) * 2 + core)
                parts[half, step].wait_recv()
                sum_send[half, step - 1] = (
                    mine + part_pair[half, step].astype(f32)
                ).astype(bf16)
                sums[half, step] = push(
                    sum_send.at[half, step - 1], sum_recv.at[half, step - 1], sum_sem,
                    (half, step - 1), {"tp": line_at(step) * 2 + core},
                )
            own_sum[half] = down(half, me_t)

        backs = {}

        def finish(half):
            parts[half, 0].wait_recv()
            value = own_sum[half] + part_pair[half, 0].astype(f32)
            for step in range(1, lines):
                sums[half, step].wait_recv()
                value = value + sum_recv[half, step - 1].astype(f32)
            value = value.astype(bf16)
            result[pl.ds(half * half_rows, half_rows)] = value
            first = half * (experts // halves)
            if half == 0:
                returned[pl.ds(0, capacity)] = value[:capacity]
            for step in range(max(first, 1), first + experts // halves):
                rows = pl.ds(step * capacity, capacity)
                backs[step] = push(
                    result.at[rows], returned.at[rows], back_sem, (step,),
                    {"sp": lax.rem(me_s + experts - step, experts)},
                )

        forward(0)
        forward(1)
        relay(0)
        forward(2)
        relay(1)
        forward(3)
        for load in loads[:2]:
            load.wait()
        settle(0)
        settle(1)
        expand(0)
        relay(2)
        loads[2].wait()
        shrink(0)
        relay(3)
        settle(2)
        settle(3)
        expand(1)
        finish(0)
        shrink(1)
        finish(1)
        slot_index = lax.broadcasted_iota(jnp.int32, (token_count, row_total), 1)
        choose = [
            jnp.where(slot_index == at_ref[:, k : k + 1], 1.0, 0.0).astype(bf16)
            for k in range(TOPK)
        ]
        for step in range(1, experts):
            backs[step].wait_recv()
        second_sum = residual_scale * normed.astype(f32)
        back_rows = returned[...]
        for k in range(TOPK):
            second_sum = second_sum + rw_ref[:, k : k + 1] * jnp.dot(
                choose[k], back_rows, preferred_element_type=f32
            )
        out_ref[...] = normalize(second_sum, last_gain_ref[...], 1).astype(bf16)
        for copy in sent:
            copy.wait_send()

    vmem = pl.BlockSpec(memory_space=pltpu.VMEM)
    hbm = pl.BlockSpec(memory_space=pl.ANY)
    dma = pltpu.SemaphoreType.DMA
    other = max(lines - 1, 1)
    return pl.pallas_call(
        kernel,
        out_shape=jax.ShapeDtypeStruct((token_count, width), bf16),
        in_specs=[vmem] * 7 + [hbm] * 3 + [vmem],
        out_specs=vmem,
        scratch_shapes=[
            pltpu.VMEM(gate_weight.shape[1:], bf16),
            pltpu.VMEM(up_weight.shape[1:], bf16),
            pltpu.VMEM(down_weight.shape[1:], bf16),
            dma((3,)),
            pltpu.VMEM((lines, token_count, width), bf16),
            pltpu.VMEM((lines, token_count, width), bf16),
            pltpu.VMEM((other, token_count, width), bf16),
            pltpu.VMEM((other, token_count, width), bf16),
            dma((2, lines)),
            dma((2, other)),
            pltpu.VMEM((2, 8, token_count), f32),
            pltpu.VMEM((2, shards - 1, 8, token_count), f32),
            dma((2, 2, shards - 1)),
            pltpu.VMEM((row_total, width), bf16),
            pltpu.VMEM((shards, row_total, width), bf16),
            dma((2, experts)),
            dma((2, groups)),
            dma((2, groups, other)),
            dma((2, groups, other)),
            pltpu.VMEM((row_total, hidden_units), bf16),
            pltpu.VMEM((halves, lines, half_rows, width), bf16),
            pltpu.VMEM((halves, lines, half_rows, width), bf16),
            pltpu.VMEM((halves, other, half_rows, width), bf16),
            pltpu.VMEM((halves, other, half_rows, width), bf16),
            pltpu.VMEM((halves, half_rows, width), f32),
            dma((2, halves, lines)),
            dma((2, halves, other)),
            pltpu.VMEM((row_total, width), bf16),
            pltpu.VMEM((row_total, width), bf16),
            dma((2, experts)),
        ],
        compiler_params=pltpu.CompilerParams(
            collective_id=1, has_side_effects=True, vmem_limit_bytes=50 << 20
        ),
    )(
        attended, out_weight, residual, norm_gain.reshape(1, -1), places, places_across,
        route_weights, gate_weight, up_weight, down_weight, final_gain.reshape(1, -1),
    )


def per_device(
    queries,
    projected_key_rows,
    projected_value_rows,
    query_gain,
    key_norm_gain,
    residual,
    out_weight,
    norm_gain,
    expert_ids,
    route_weights,
    gate_weight,
    up_weight,
    down_weight,
    final_gain,
):
    token_count = queries.shape[0]
    query_heads = queries.shape[1] // HEAD_DIM
    key_heads = projected_key_rows.shape[1] // HEAD_DIM
    queries_per_group = query_heads // key_heads
    token_positions = lax.axis_index("sp") * token_count + jnp.arange(token_count, dtype=jnp.int32)
    queries_after_rotation = rotary_over_grid(
        normalize_heads(queries, query_gain, query_heads), token_positions
    ).astype(jnp.bfloat16)
    keys_after_rotation = rotary_over_grid(
        normalize_heads(projected_key_rows, key_norm_gain, key_heads), token_positions
    ).astype(jnp.bfloat16)
    packed = jnp.concatenate(
        [keys_after_rotation, projected_value_rows.reshape(token_count, key_heads, HEAD_DIM)], -1
    ).reshape(token_count, key_heads * 2 * HEAD_DIM)
    grouped_query_heads = (
        queries_after_rotation.reshape(token_count, key_heads, queries_per_group, HEAD_DIM)
        .transpose(1, 2, 0, 3)
        .reshape(key_heads, queries_per_group * token_count, HEAD_DIM)
    )
    score_scale = HEAD_DIM ** (-0.5)
    query_total = queries_per_group * token_count
    group = lax.axis_size("sp")
    section = ring_gather(packed, group, 1 << ((group.bit_length() - 1) // 2)).reshape(
        group * token_count, packed.shape[1]
    )
    running_max = jnp.full((key_heads, query_total), far_below, jnp.float32)
    opened = section.reshape(section.shape[0], key_heads, 2 * HEAD_DIM)
    scores = (
        jnp.einsum(
            "hqd,khd->hqk",
            grouped_query_heads,
            opened[:, :, :HEAD_DIM],
            preferred_element_type=jnp.float32,
        )
        * score_scale
    )
    new_peak = jnp.maximum(running_max, jnp.max(scores, -1))
    weights = jnp.exp(scores - new_peak[:, :, None])
    running_sum = jnp.sum(weights, -1)
    running_out = jnp.einsum(
        "hqk,khd->hqd",
        weights.astype(jnp.bfloat16),
        opened[:, :, HEAD_DIM:],
        preferred_element_type=jnp.float32,
    )
    running_max, running_sum, running_out = (new_peak, running_sum, running_out)
    attended = (running_out / running_sum[:, :, None]).astype(jnp.bfloat16)
    attended = (
        attended.reshape(key_heads, queries_per_group, token_count, HEAD_DIM)
        .transpose(2, 0, 1, 3)
        .reshape(token_count, query_heads * HEAD_DIM)
    )
    expert_count = group
    capacity = 4 * token_count // expert_count
    flat_ids = expert_ids.reshape(-1)
    marked = (flat_ids[:, None] == jnp.arange(expert_count, dtype=jnp.int32)[None, :]).astype(
        jnp.int32
    )
    earlier = jnp.cumsum(marked, 0) - marked
    away = lax.rem(flat_ids - lax.axis_index("sp") + expert_count, expert_count)
    places = (away * capacity + jnp.sum(earlier * marked, 1)).reshape(token_count, TOPK)
    return after_attention(
        attended,
        out_weight,
        residual,
        norm_gain,
        places,
        route_weights,
        gate_weight,
        up_weight,
        down_weight,
        final_gain,
        expert_count,
        lax.axis_size("tp"),
    )


def solution(mesh):
    in_specs = (
        P("sp", "tp"),
        P("sp", "tp"),
        P("sp", "tp"),
        P(),
        P(),
        P("sp", "tp"),
        P("tp", None),
        P("tp"),
        P("sp", None),
        P("sp", None),
        P("sp", None, "tp"),
        P("sp", None, "tp"),
        P("sp", "tp", None),
        P("tp"),
    )
    out_specs = P("sp", "tp")
    return jax.shard_map(
        per_device, mesh=mesh, in_specs=in_specs, out_specs=out_specs, check_vma=False
    )
```

time: 210 us -> 96 us (0.46)
  waiting for transfers between devices: 126 us -> 0 us
  Pallas kernels: 0 us -> 84.9 us
  blocking collectives: 31.5 us -> 0 us
  matrix products: 23.2 us -> 1.85 us
  between operations: 13.4 us -> 0.29 us
  starting transfers between devices: 5.64 us -> 0 us
  other arithmetic: 5.31 us -> 2.79 us
    pallas_call x0 -> x2, Pallas kernels: none -> 84.9 us  [the longest x1 65.3 us: after_attention(): pl.pallas_call(kernel, out_shape=jax.ShapeDtypeStruct((token_count, width...]
    all_gather x2 -> x0, waiting for transfers between devices: 61.2 us -> none  [the longest x1 40.3 us: per_device(): section = lax.all_gather(packed, 'sp', axis=0, tiled=True)]
    reduce_scatter x2 -> x0, waiting for transfers between devices: 50.6 us -> none  [the longest x1 31.3 us: per_device(): lax.psum_scatter(lax.dot_general(columns, hidden, (((0,), (1,)), ((), ())...]
    dot_general x6 -> x0, matrix products: 20.3 us -> none  [the longest x1 10.6 us: per_device(): lax.dot_general(columns, hidden, (((0,), (1,)), ((), ())), preferred_elem...]
    all_to_all x1 -> x0, blocking collectives: 19.8 us -> none  [per_device(): lax.all_to_all(outgoing.reshape(expert_count, capacity, local_width), 'sp...]
    all_to_all x1 -> x0, waiting for transfers between devices: 14.3 us -> none  [per_device(): lax.all_to_all(expert_out.reshape(local_width, expert_count, capacity), '...]
    psum x2 -> x0, blocking collectives: 11.7 us -> none  [norm_features(): row_sums, squares = lax.psum((row_sums, squares), 'tp')]
    all_to_all x1 -> x0, starting transfers between devices: 5.51 us -> none  [per_device(): lax.all_to_all(expert_out.reshape(local_width, expert_count, capacity), '...]
  transfers between devices with their start and end apart: 5 -> 0, of which waited for: 5 -> 0; matrix products, arithmetic and copies ran while one was open for 2% -> 0% of each run, Pallas kernels for 0% -> 0%
where the time goes in v1:
time: 96 us; the launch traced here: 95.8 us
  Pallas kernels  84.9 us (88%)
  local copies, waits for them, and re-layouts  5.94 us (6%)
  other arithmetic  2.79 us (3%)
  matrix products  1.85 us (2%)
    pallas_call x1, Pallas kernels, after_attention(): pl.pallas_call(kernel, out_shape=jax.ShapeDtypeStruct((token_count, width...  65.3 us
    pallas_call x1, Pallas kernels, ring_gather(): pl.pallas_call(kernel, out_shape=jax.ShapeDtypeStruct((group, rows, width...  19.6 us
    unnamed x20, local copies, waits for them, and re-layouts  3.63 us

profile of v1, /device:TPU:0, one launch (start us, length us, event | category | flops | bytes accessed | tf_op | source)
XLA Modules:
  0.0 95.8 jit_solution(9036886041914912669)
XLA Ops:
  0.0 0.1 multiply_cosine_fusion
  0.2 1.0 copy.22
  1.2 0.7 fusion.21
  2.0 1.0 copy.23
  3.0 0.1 copy.34.mine_ref
  3.1 19.6 %shard_map.136 = bf16[8,128,512]{2,1,0:T(8,128)(2,1)S(1)} custom-call(bf16[128,512]{1,0:T(8,128)(2,1)S(1)} %copy.34.mine_ref), custom_call_target="tpu_custom_call" | custom-call | tf_op jit(solution)/shard_map/pallas_call | solution.py:129
  22.7 0.3 reshape_reshape.3
  23.0 0.9 fusion.37
  24.0 0.1 copy.20
  24.3 0.9 multiply_reduce_fusion
  25.2 0.9 fusion
  26.1 1.0 %fusion.12 = bf16[4,8,2,8,128]{4,3,2,1,0:T(8,128)(2,1)S(1)} fusion(f32[4,256,1024]{2,1,0:T(8,128)S(1)} %get-tuple-element.20, f32[4,256]{1,0:T(4,128)S(1)} %broadcast_maximum_fusion, bf16[1024,4,64]{2,1,0:T(4,128)(2,1)S(1)} %get-tuple-element.5, f32[4,256]{1,0:T(4,128)S(1)} %fusion), kind=kOutput, calls=%fused_computation.9 | convolution fusion | flops 137494528 | bytes 4857856 | tf_op jit(solution)/shard_map/hqk,khd->hqd/dot_general | solution.py:524
  27.2 0.1 copy.31.att_ref
  27.3 0.1 copy.28
  27.4 0.1 eq.32
  27.6 0.6 reduce-window.6
  28.1 0.2 slice_reduce_fusion
  28.4 0.1 eq.28
  28.5 0.1 fusion.29
  28.6 0.1 reduce_sum.42
  28.9 0.1 copy.32.at_ref
  29.0 0.8 copy.33.rw_ref
  29.8 65.3 %shard_map.137 = bf16[128,512]{1,0:T(8,128)(2,1)S(1)} custom-call(bf16[128,512]{1,0:T(8,128)(2,1)S(1)} %copy.31.att_ref, bf16[512,2048]{1,0:T(8,128)(2,1)S(1)} %copy-done, bf16[128,512]{1,0:T(8,128)(2,1)S(1)} %copy-done.1, f32[1,512]{1,0:T(1,128)S(1)} %bitcast.44, s32[128,2]{1,0:T(8,128)S(1)} %copy.32.at_ref, s32[2,128]{1,0:T(2,128)S(1)} %bitcast.43, ...), custom_call_target="tpu_custom_call" | custom-call | tf_op jit(solution)/shard_map/pallas_call | solution.py:423
  95.2 0.7 copy.58
  (34 shorter events, 0.5 us)
Async XLA Ops:
  1.9 22.1 %copy-start.4 = (bf16[128,512]{1,0:T(8,128)(2,1)S(1)}, bf16[128,512]{1,0:T(8,128)(2,1)}, u32[]{:S(2)}) copy-start(bf16[128,512]{1,0:T(8,128)(2,1)} %param.14) | copy-start | bytes 393220
  2.0 22.2 %copy-start.6 = (f32[64]{0:T(128)S(1)}, f32[64]{0:T(128)}, u32[]{:S(2)}) copy-start(f32[64]{0:T(128)} %param.17) | copy-start | bytes 772
  26.1 1.2 %copy-start.5 = (s32[128,2]{0,1:T(2,128)S(1)}, s32[128,2]{0,1:T(2,128)}, u32[]{:S(2)}) copy-start(s32[128,2]{0,1:T(2,128)} %param.22) | copy-start | bytes 3076
  26.1 3.7 %copy-start = (bf16[512,2048]{1,0:T(8,128)(2,1)S(1)}, bf16[512,2048]{1,0:T(8,128)(2,1)}, u32[]{:S(2)}) copy-start(bf16[512,2048]{1,0:T(8,128)(2,1)} %ow_ref.1) | copy-start | bytes 6291460
  26.1 3.7 %copy-start.1 = (bf16[128,512]{1,0:T(8,128)(2,1)S(1)}, bf16[128,512]{1,0:T(8,128)(2,1)}, u32[]{:S(2)}) copy-start(bf16[128,512]{1,0:T(8,128)(2,1)} %res_ref.1) | copy-start | bytes 393220
  26.1 3.7 %copy-start.2 = (f32[512]{0:T(512)S(1)}, f32[512]{0:T(512)}, u32[]{:S(2)}) copy-start(f32[512]{0:T(512)} %param.21) | copy-start | bytes 6148
  26.1 3.7 %copy-start.3 = (f32[512]{0:T(512)S(1)}, f32[512]{0:T(512)}, u32[]{:S(2)}) copy-start(f32[512]{0:T(512)} %param.27) | copy-start | bytes 6148

commit v2 on v1

--- a/solution.py
+++ b/solution.py
@@ -153,7 +153,7 @@
     groups = 4
     group_rows = row_total // groups
     group_experts = experts // groups
-    halves = 2
+    halves = groups
     half_rows = row_total // halves
     hidden_units = gate_weight.shape[2]
     tile = min(256, hidden_units)
@@ -168,7 +168,7 @@
         mix_send, mix_pair, line_send, line_recv, mix_sem, line_sem,
         stat_send, stat_recv, stat_sem,
         outgoing, routed, out_sem, fwd_sem, cross_sem, relay_sem,
-        hidden, part_send, part_pair, sum_send, sum_recv, own_sum, part_sem, sum_sem,
+        hidden, part_send, part_pair, sum_send, sum_recv, own_sum, other_sum, part_sem, sum_sem,
         result, returned, back_sem,
     ):
         me_s = lax.axis_index("sp")
@@ -347,16 +347,19 @@
                     {"tp": partner},
                 )
             for step in range(1, lines):
-                mine = down(half, line_at(step) * 2 + core)
+                other_sum[half, step - 1] = down(half, line_at(step) * 2 + core)
+            own_sum[half] = down(half, me_t)
+
+        def join(half):
+            for step in range(1, lines):
                 parts[half, step].wait_recv()
                 sum_send[half, step - 1] = (
-                    mine + part_pair[half, step].astype(f32)
+                    other_sum[half, step - 1] + part_pair[half, step].astype(f32)
                 ).astype(bf16)
                 sums[half, step] = push(
                     sum_send.at[half, step - 1], sum_recv.at[half, step - 1], sum_sem,
                     (half, step - 1), {"tp": line_at(step) * 2 + core},
                 )
-            own_sum[half] = down(half, me_t)
 
         backs = {}
 
@@ -381,24 +384,34 @@
         forward(0)
         forward(1)
         relay(0)
-        forward(2)
-        relay(1)
-        forward(3)
         for load in loads[:2]:
             load.wait()
         settle(0)
-        settle(1)
         expand(0)
-        relay(2)
+        forward(2)
+        relay(1)
         loads[2].wait()
         shrink(0)
+        forward(3)
+        settle(1)
+        join(0)
+        expand(1)
+        relay(2)
+        shrink(1)
+        settle(2)
+        join(1)
+        finish(0)
+        expand(2)
         relay(3)
-        settle(2)
+        shrink(2)
         settle(3)
-        expand(1)
-        finish(0)
-        shrink(1)
+        join(2)
         finish(1)
+        expand(3)
+        shrink(3)
+        join(3)
+        finish(2)
+        finish(3)
         slot_index = lax.broadcasted_iota(jnp.int32, (token_count, row_total), 1)
         choose = [
             jnp.where(slot_index == at_ref[:, k : k + 1], 1.0, 0.0).astype(bf16)
@@ -451,6 +464,7 @@
             pltpu.VMEM((halves, other, half_rows, width), bf16),
             pltpu.VMEM((halves, other, half_rows, width), bf16),
             pltpu.VMEM((halves, half_rows, width), f32),
+            pltpu.VMEM((halves, other, half_rows, width), f32),
             dma((2, halves, lines)),
             dma((2, halves, other)),
             pltpu.VMEM((row_total, width), bf16),
@@ -536,13 +550,17 @@
     )
     expert_count = group
     capacity = 4 * token_count // expert_count
-    flat_ids = expert_ids.reshape(-1)
-    marked = (flat_ids[:, None] == jnp.arange(expert_count, dtype=jnp.int32)[None, :]).astype(
-        jnp.int32
-    )
-    earlier = jnp.cumsum(marked, 0) - marked
-    away = lax.rem(flat_ids - lax.axis_index("sp") + expert_count, expert_count)
-    places = (away * capacity + jnp.sum(earlier * marked, 1)).reshape(token_count, TOPK)
+    marked = (
+        expert_ids[:, :, None] == jnp.arange(expert_count, dtype=jnp.int32)[None, None, :]
+    ).astype(jnp.float32)
+    token_index = jnp.arange(token_count, dtype=jnp.int32)
+    before = (token_index[None, :] < token_index[:, None]).astype(jnp.bfloat16)
+    earlier = jnp.dot(
+        before, jnp.sum(marked, 1).astype(jnp.bfloat16), preferred_element_type=jnp.float32
+    )
+    slots = jnp.sum(earlier[:, None, :] * marked, 2).astype(jnp.int32)
+    away = lax.rem(expert_ids - lax.axis_index("sp") + expert_count, expert_count)
+    places = away * capacity + slots
     return after_attention(
         attended,
         out_weight,

time: 96 us -> 87.9 us (0.916)
  Pallas kernels: 84.9 us -> 78.9 us
  local copies, waits for them, and re-layouts: 5.94 us -> 4.46 us
    pallas_call x1, Pallas kernels: 65.3 us -> 59.3 us  [after_attention(): pl.pallas_call(kernel, out_shape=jax.ShapeDtypeStruct((token_count, width...]
    unnamed x20 -> x21, local copies, waits for them, and re-layouts: 3.63 us -> 2.84 us
where the time goes in v2:
time: 87.9 us; the launch traced here: 87.7 us
  Pallas kernels  78.9 us (90%)
  local copies, waits for them, and re-layouts  4.46 us (5%)
  other arithmetic  2.1 us (2%)
  matrix products  1.94 us (2%)
    pallas_call x1, Pallas kernels, after_attention(): pl.pallas_call(kernel, out_shape=jax.ShapeDtypeStruct((token_count, width...  59.3 us
    pallas_call x1, Pallas kernels, ring_gather(): pl.pallas_call(kernel, out_shape=jax.ShapeDtypeStruct((group, rows, width...  19.6 us
    unnamed x21, local copies, waits for them, and re-layouts  2.84 us

profile of v2, /device:TPU:0, one launch (start us, length us, event | category | flops | bytes accessed | tf_op | source)
XLA Modules:
  0.0 87.7 jit_solution(16024964141219164396)
XLA Ops:
  0.0 0.1 multiply_cosine_fusion
  0.2 1.0 %copy.37 = bf16[128,256]{0,1:T(8,128)(2,1)S(1)} copy(bf16[128,256]{1,0:T(8,128)(2,1)} %param.15) | data formatting | bytes 131072 | tf_op args[1]
  1.2 0.7 fusion.21
  1.9 0.0 copy-start.4
  2.0 0.0 copy-start.7
  2.0 1.0 %copy.38 = bf16[128,256]{0,1:T(8,128)(2,1)S(1)} copy(bf16[128,256]{1,0:T(8,128)(2,1)} %param.16) | data formatting | bytes 131072 | tf_op args[2]
  3.0 0.1 copy.46.mine_ref
  3.1 19.6 %shard_map.136 = bf16[8,128,512]{2,1,0:T(8,128)(2,1)S(1)} custom-call(bf16[128,512]{1,0:T(8,128)(2,1)S(1)} %copy.46.mine_ref), custom_call_target="tpu_custom_call" | custom-call | tf_op jit(solution)/shard_map/pallas_call | solution.py:129
  22.7 0.3 reshape_reshape.3
  23.0 0.9 %fusion.36 = (bf16[1024,4,64]{2,1,0:T(4,128)(2,1)S(1)}, bf16[1024,4,64]{2,1,0:T(4,128)(2,1)S(1)}) fusion(bf16[1024,4,128]{2,1,0:T(4,128)(2,1)S(1)} %reshape_reshape.3), kind=kLoop, calls=%fused_computation.66 | loop fusion | bytes 2097152 | tf_op jit(solution)/shard_map/slice | solution.py:541
  24.0 0.1 copy.35
  24.2 0.1 fusion.19
  24.3 0.9 multiply_reduce_fusion
  25.2 0.9 %fusion = f32[4,256]{1,0:T(4,128)S(1)} fusion(f32[4,256,1024]{2,1,0:T(8,128)S(1)} %get-tuple-element.20, f32[4,256]{1,0:T(4,128)S(1)} %broadcast_maximum_fusion), kind=kLoop, calls=%fused_computation.2 | loop fusion | flops 3144704 | bytes 4202496 | tf_op jit(solution)/shard_map/reduce_sum | solution.py:537
  26.1 0.0 copy-start.6
  26.1 0.0 copy-start.1
  26.1 0.0 copy-start.2
  26.1 1.0 %fusion.12 = bf16[4,8,2,8,128]{4,3,2,1,0:T(8,128)(2,1)S(1)} fusion(f32[4,256,1024]{2,1,0:T(8,128)S(1)} %get-tuple-element.20, f32[4,256]{1,0:T(4,128)S(1)} %broadcast_maximum_fusion, bf16[1024,4,64]{2,1,0:T(4,128)(2,1)S(1)} %get-tuple-element.5, f32[4,256]{1,0:T(4,128)S(1)} %fusion), kind=kOutput, calls=%fused_computation.9 | convolution fusion | flops 137494528 | bytes 4857856 | tf_op jit(solution)/shard_map/hqk,khd->hqd/dot_general | solution.py:538
  27.1 0.1 copy.43.att_ref
  27.3 0.1 fusion.24
  27.5 0.1 copy.44.at_ref
  27.6 0.1 copy.45.rw_ref
  27.7 59.3 %shard_map.137 = bf16[128,512]{1,0:T(8,128)(2,1)S(1)} custom-call(bf16[128,512]{1,0:T(8,128)(2,1)S(1)} %copy.43.att_ref, bf16[512,2048]{1,0:T(8,128)(2,1)S(1)} %copy-done, bf16[128,512]{1,0:T(8,128)(2,1)S(1)} %copy-done.1, f32[1,512]{1,0:T(1,128)S(1)} %bitcast.37, s32[128,2]{1,0:T(8,128)S(1)} %copy.44.at_ref, s32[2,128]{1,0:T(2,128)S(1)} %bitcast.36, ...), custom_call_target="tpu_custom_call" | custom-call | tf_op jit(solution)/shard_map/pallas_call | solution.py:436
  87.0 0.7 copy.70
  (28 shorter events, 0.3 us)
Async XLA Ops:
  1.9 22.1 %copy-start.4 = (bf16[128,512]{1,0:T(8,128)(2,1)S(1)}, bf16[128,512]{1,0:T(8,128)(2,1)}, u32[]{:S(2)}) copy-start(bf16[128,512]{1,0:T(8,128)(2,1)} %param.14) | copy-start | bytes 393220
  2.0 22.2 %copy-start.7 = (f32[64]{0:T(128)S(1)}, f32[64]{0:T(128)}, u32[]{:S(2)}) copy-start(f32[64]{0:T(128)} %param.17) | copy-start | bytes 772
  26.1 1.2 %copy-start.5 = (s32[128,2]{0,1:T(2,128)S(1)}, s32[128,2]{0,1:T(2,128)}, u32[]{:S(2)}) copy-start(s32[128,2]{0,1:T(2,128)} %param.22) | copy-start | bytes 3076
  26.1 1.5 %copy-start.6 = (f32[128,2]{0,1:T(2,128)S(1)}, f32[128,2]{0,1:T(2,128)}, u32[]{:S(2)}) copy-start(f32[128,2]{0,1:T(2,128)} %param.23) | copy-start | bytes 3076
  26.1 1.6 %copy-start = (bf16[512,2048]{1,0:T(8,128)(2,1)S(1)}, bf16[512,2048]{1,0:T(8,128)(2,1)}, u32[]{:S(2)}) copy-start(bf16[512,2048]{1,0:T(8,128)(2,1)} %ow_ref.1) | copy-start | bytes 6291460
  26.1 1.6 %copy-start.1 = (bf16[128,512]{1,0:T(8,128)(2,1)S(1)}, bf16[128,512]{1,0:T(8,128)(2,1)}, u32[]{:S(2)}) copy-start(bf16[128,512]{1,0:T(8,128)(2,1)} %res_ref.1) | copy-start | bytes 393220
  26.1 1.6 %copy-start.2 = (f32[512]{0:T(512)S(1)}, f32[512]{0:T(512)}, u32[]{:S(2)}) copy-start(f32[512]{0:T(512)} %param.21) | copy-start | bytes 6148
  26.1 1.6 %copy-start.3 = (f32[512]{0:T(512)S(1)}, f32[512]{0:T(512)}, u32[]{:S(2)}) copy-start(f32[512]{0:T(512)} %param.27) | copy-start | bytes 6148
